TPU v7x, 32 devices: a whole 2x2x4 slice. The times are simulated.
32 devices in a mesh: ep: 8 (over z, x), tp: 4 (over y, core).
Axes of the slice: x: 2, y: 2, z: 4, core: 2. Of those that a mesh axis runs over, the one named last changes fastest.
Arguments:
- mixer_group_input: bfloat16 [2048, 1024], P('ep', 'tp'), may hold values from -6 to 6
- log_step_size: float32 [64, 2048], P('tp', 'ep'), may hold values from -16 to 0
- extra_log_decay: float32 [64, 2048], P('tp', 'ep'), may hold values from -0.7 to 0
- negated_eigen_real: float32 [64, 64], P('tp'), may hold values from 0.35 to 0.7
- frequency: float32 [64, 64], P('tp'), may hold values from 0 to 200
- group_input_matrices: bfloat16 [2, 64, 64, 16], P(None, 'tp'), may hold values from -1.5 to 1.5
- group_output_matrices: bfloat16 [2, 64, 16, 64], P(None, 'tp'), may hold values from -0.5 to 0.5
- channel_feedthrough: float32 [1024], P('tp'), may hold values from -3 to 3
- mixer_norm_scale: float32 [1024], replicated, may hold values from 0.1 to 1.9
- mixer_output_weight: bfloat16 [1024, 2048], P(None, 'tp'), may hold values from -0.1875 to 0.1875
- second_micro_input: bfloat16 [1024, 2048], P('ep'), may hold values from -6 to 6
- expert_norm_scale: float32 [2048], replicated, may hold values from 0.1 to 1.9
- routes: int32 [1024, 4], P('ep'), may hold values from 0 to 7, all different within a row; in each aligned block of 128 rows (0 to 127, 128 to 255, ...) at most 128 rows name the same one
- chosen_expert_weight: float32 [1024, 4], P('ep'), may hold values from 0.1 to 1
- expert_gate_weight: bfloat16 [8, 2048, 2048], P('ep', None, 'tp'), may hold values from -0.125 to 0.125
- expert_up_weight: bfloat16 [8, 2048, 2048], P('ep', None, 'tp'), may hold values from -0.125 to 0.125
- expert_down_weight: bfloat16 [8, 2048, 2048], P('ep', None, 'tp'), may hold values from -0.125 to 0.125
- shared_gate_weight: bfloat16 [2048, 2048], P(None, 'tp'), may hold values from -0.125 to 0.125
- shared_up_weight: bfloat16 [2048, 2048], P(None, 'tp'), may hold values from -0.125 to 0.125
- shared_down_weight: bfloat16 [2048, 2048], P(None, 'tp'), may hold values from -0.125 to 0.125
Outputs:
- mixed: bfloat16 [2048, 2048], P('ep', 'tp')
- moe_out: bfloat16 [1024, 2048], P('ep', 'tp')
Inputs may be any that keep to these rules, and one draw needn't show every extreme that they name: `routes`: each row names 4 different experts; in each aligned block of 128 rows no expert is named by more than 128 rows, and in some block one expert is named by exactly 128 rows.
All inputs are finite; a program needn't handle non-finite values.
Results may differ from a plain program's by a relative error of at most 0.0068.
Values may be sent and summed in bfloat16 or wider, within the bound.
A program may use at most 192 MiB of HBM per device.

v0:
```python
import jax
import jax.numpy as jnp
from jax import lax
from jax.sharding import PartitionSpec as P

eps_norm = 1e-06


def entering(part, axis, combine, identity):
    place = lax.axis_index(axis)
    gathered = jax.tree.map(lambda a: lax.all_gather(a, axis), part)
    state = jax.tree.map(lambda a, e: jnp.zeros_like(a) + jnp.asarray(e, a.dtype), part, identity)

    def one(hop, state):
        return combine(
            state, jax.tree.map(lambda a: lax.dynamic_index_in_dim(a, hop, 0, False), gathered)
        )

    return lax.fori_loop(0, place, one, state)


def combine_steps(earlier, latter):
    return (
        earlier[0] * latter[0] - earlier[1] * latter[1],
        earlier[0] * latter[1] + earlier[1] * latter[0],
        latter[0] * earlier[2] - latter[1] * earlier[3] + latter[2],
        latter[0] * earlier[3] + latter[1] * earlier[2] + latter[3],
    )


def local_states(inputs, step_logs, losses, negated_eigen_real, frequency, group_input_matrices):
    positions = inputs.shape[0]
    group_list, states = negated_eigen_real.shape
    channels = inputs.reshape(positions, group_list, -1)
    step_size = jnp.exp(step_logs).T
    decay_log = -negated_eigen_real[None, :, :] * step_size[:, :, None]
    magnitude = jnp.exp(decay_log + losses.T[:, :, None])
    rotation = frequency[None, :, :] * step_size[:, :, None]
    scaling = jnp.sqrt(-jnp.expm1(2.0 * decay_log))
    driven = jnp.einsum(
        "tgc,rgpc->rtgp", channels, group_input_matrices, preferred_element_type=jnp.float32
    )
    operands = (
        magnitude * jnp.cos(rotation),
        magnitude * jnp.sin(rotation),
        scaling * driven[0],
        scaling * driven[1],
    )
    flat_operands = tuple((item.reshape(positions, group_list * states) for item in operands))
    scanned = lax.associative_scan(combine_steps, flat_operands, axis=0)
    return tuple((item.reshape(positions, group_list, states) for item in scanned))


def readout(state_real_part, state_imaginary, group_output_matrices, inputs, channel_feedthrough):
    positions = state_real_part.shape[0]
    mapped_result = jnp.einsum(
        "fnx,njx->fnj",
        state_real_part,
        group_output_matrices[0].astype(jnp.float32),
        precision=lax.Precision.HIGHEST,
    )
    mapped_result = mapped_result - jnp.einsum(
        "fnx,njx->fnj",
        state_imaginary,
        group_output_matrices[1].astype(jnp.float32),
        precision=lax.Precision.HIGHEST,
    )
    total = mapped_result.reshape(positions, -1) + channel_feedthrough * inputs.astype(jnp.float32)
    return jax.nn.gelu(total).astype(jnp.bfloat16)


def scaled_rows(values, gain):
    widened = values.astype(jnp.float32)
    factor = lax.rsqrt(jnp.mean(widened * widened, axis=-1, keepdims=True) + eps_norm)
    return (widened * factor * gain).astype(jnp.bfloat16)


def slot_table(block_routes, experts, capacity):
    flat_routes = block_routes.reshape(-1)
    onehot = (flat_routes[:, None] == jnp.arange(experts, dtype=jnp.int32)[None, :]).astype(
        jnp.int32
    )
    earlier_count = jnp.sum((jnp.cumsum(onehot, axis=0) - onehot) * onehot, axis=1)
    return flat_routes * capacity + earlier_count


def fill_slots(token_rows, slot_index, slot_count, top_count):
    owner_row = (
        jnp.zeros((slot_count,), jnp.int32)
        .at[slot_index]
        .set(jnp.arange(slot_index.shape[0], dtype=jnp.int32) // top_count)
    )
    occupied = jnp.zeros((slot_count,), jnp.int32).at[slot_index].set(1)
    return jnp.where(occupied[:, None] > 0, token_rows[owner_row], jnp.zeros((), token_rows.dtype))


def on_device(
    mixer_group_input,
    log_step_size,
    extra_log_decay,
    negated_eigen_real,
    frequency,
    group_input_matrices,
    group_output_matrices,
    channel_feedthrough,
    mixer_norm_scale,
    mixer_output_weight,
    second_micro_input,
    expert_norm_scale,
    routes,
    chosen_expert_weight,
    expert_gate_weight,
    expert_up_weight,
    expert_down_weight,
    shared_gate_weight,
    shared_up_weight,
    shared_down_weight,
):
    reach_real, reach_imag, state_real_part, state_imaginary = local_states(
        mixer_group_input,
        log_step_size,
        extra_log_decay,
        negated_eigen_real,
        frequency,
        group_input_matrices,
    )
    block_ends = (reach_real[-1], reach_imag[-1], state_real_part[-1], state_imaginary[-1])
    identity = (
        jnp.ones_like(block_ends[0]),
        jnp.zeros_like(block_ends[1]),
        jnp.zeros_like(block_ends[2]),
        jnp.zeros_like(block_ends[3]),
    )
    prefix = entering(block_ends, "ep", combine_steps, identity)
    state_real_part = state_real_part + reach_real * prefix[2] - reach_imag * prefix[3]
    state_imaginary = state_imaginary + reach_real * prefix[3] + reach_imag * prefix[2]
    ssm_out = readout(
        state_real_part,
        state_imaginary,
        group_output_matrices,
        mixer_group_input,
        channel_feedthrough,
    )
    whole_rows = lax.all_gather(ssm_out, "tp", axis=1, tiled=True)
    normed_mix = scaled_rows(whole_rows, mixer_norm_scale)
    mixed = jnp.dot(normed_mix, mixer_output_weight, preferred_element_type=jnp.float32).astype(
        jnp.bfloat16
    )
    token_count, top_count = routes.shape
    model_width = second_micro_input.shape[1]
    experts = lax.axis_size("ep")
    capacity = 2 * token_count * top_count // experts
    slot_count = experts * capacity
    column_count = expert_down_weight.shape[2]
    gate_weight = expert_gate_weight[0]
    up_weight = expert_up_weight[0]
    down_weight = expert_down_weight[0]
    normed_tokens = scaled_rows(second_micro_input, expert_norm_scale)
    slot_index = slot_table(routes, experts, capacity)
    sent = fill_slots(normed_tokens, slot_index, slot_count, top_count).reshape(
        experts, capacity, model_width
    )
    arrived = lax.all_to_all(sent, "ep", split_axis=0, concat_axis=0, tiled=True).reshape(
        slot_count, model_width
    )
    gate_part = jnp.dot(arrived, gate_weight, preferred_element_type=jnp.float32)
    up_part = jnp.dot(arrived, up_weight, preferred_element_type=jnp.float32)
    hidden = (jax.nn.silu(gate_part) * up_part).astype(jnp.bfloat16)
    shared_hidden = (
        jax.nn.silu(jnp.dot(normed_tokens, shared_gate_weight, preferred_element_type=jnp.float32))
        * jnp.dot(normed_tokens, shared_up_weight, preferred_element_type=jnp.float32)
    ).astype(jnp.bfloat16)
    routed_columns = jnp.dot(
        lax.all_gather(hidden, "tp", axis=1, tiled=True),
        down_weight,
        preferred_element_type=jnp.float32,
    )
    shared_columns = jnp.dot(
        lax.all_gather(shared_hidden, "tp", axis=1, tiled=True),
        shared_down_weight,
        preferred_element_type=jnp.float32,
    )
    results = routed_columns.astype(jnp.bfloat16).reshape(experts, capacity, column_count)
    returned = lax.all_to_all(results, "ep", split_axis=0, concat_axis=0, tiled=True).reshape(
        slot_count, column_count
    )
    picked = returned[slot_index].reshape(token_count, top_count, column_count).astype(jnp.float32)
    moe_out = (shared_columns + jnp.sum(picked * chosen_expert_weight[:, :, None], axis=1)).astype(
        jnp.bfloat16
    )
    return (mixed, moe_out)


def solution(mesh):
    return jax.shard_map(
        on_device,
        mesh=mesh,
        in_specs=(
            P("ep", "tp"),
            P("tp", "ep"),
            P("tp", "ep"),
            P("tp", None),
            P("tp", None),
            P(None, "tp", None, None),
            P(None, "tp", None, None),
            P("tp"),
            P(),
            P(None, "tp"),
            P("ep", None),
            P(),
            P("ep", None),
            P("ep", None),
            P("ep", None, "tp"),
            P("ep", None, "tp"),
            P("ep", None, "tp"),
            P(None, "tp"),
            P(None, "tp"),
            P(None, "tp"),
        ),
        out_specs=(P("ep", "tp"), P("ep", "tp")),
        check_vma=False,
    )
```

profile of v0, /device:TPU:0, one launch (start us, length us, event | category | flops | bytes accessed | tf_op | source)
XLA Modules:
  0.0 1486.9 jit_solution(2442803087446113709)
XLA Ops:
  28.7 7.4 all-to-all-start
  39.4 8.7 fusion.35
  48.1 20.7 %slice.519 = f32[128,1024]{0,1:T(8,128)} slice(f32[256,1024]{0,1:T(8,128)} %get-tuple-element.228), slice={[0:255:2], [0:1024:1]} | slice | bytes 1048576 | tf_op jit(solution)/shard_map/slice | solution.py:50
  68.7 20.7 %slice.523 = f32[128,1024]{0,1:T(8,128)} slice(f32[256,1024]{0,1:T(8,128)} %get-tuple-element.228), slice={[1:256:2], [0:1024:1]} | slice | bytes 1048576 | tf_op jit(solution)/shard_map/slice | solution.py:50
  89.4 20.7 %slice.518 = f32[128,1024]{0,1:T(8,128)} slice(f32[256,1024]{0,1:T(8,128)} %get-tuple-element.229), slice={[1:256:2], [0:1024:1]} | slice | bytes 1048576 | tf_op jit(solution)/shard_map/slice | solution.py:50
  110.1 20.7 %slice.525 = f32[128,1024]{0,1:T(8,128)} slice(f32[256,1024]{0,1:T(8,128)} %get-tuple-element.229), slice={[0:255:2], [0:1024:1]} | slice | bytes 1048576 | tf_op jit(solution)/shard_map/slice | solution.py:50
  130.7 20.9 %slice.520 = f32[128,1024]{0,1:T(8,128)} slice(f32[256,1024]{0,1:T(8,128)} %get-tuple-element.230), slice={[1:256:2], [0:1024:1]} | slice | bytes 1048576 | tf_op jit(solution)/shard_map/slice | solution.py:50
  151.6 20.7 %slice.526 = f32[128,1024]{0,1:T(8,128)} slice(f32[256,1024]{0,1:T(8,128)} %get-tuple-element.230), slice={[0:255:2], [0:1024:1]} | slice | bytes 1048576 | tf_op jit(solution)/shard_map/slice | solution.py:50
  172.2 20.7 %slice.522 = f32[128,1024]{0,1:T(8,128)} slice(f32[256,1024]{0,1:T(8,128)} %get-tuple-element.227), slice={[0:255:2], [0:1024:1]} | slice | bytes 1048576 | tf_op jit(solution)/shard_map/slice | solution.py:50
  192.9 20.7 %slice.531 = f32[128,1024]{0,1:T(8,128)} slice(f32[256,1024]{0,1:T(8,128)} %get-tuple-element.227), slice={[1:256:2], [0:1024:1]} | slice | bytes 1048576 | tf_op jit(solution)/shard_map/slice | solution.py:50
  217.1 11.6 slice.529
  228.7 11.3 slice.533
  240.0 11.3 slice.528
  251.3 10.5 slice.535
  261.8 11.4 slice.530
  273.2 11.2 slice.536
  284.4 10.5 slice.532
  294.9 11.4 slice.541
  309.8 6.6 slice.539
  316.4 6.6 slice.543
  334.8 6.7 slice.540
  341.5 6.5 slice.546
  540.7 6.5 slice.537
  547.2 6.5 slice.616
  553.7 6.5 slice.620
  560.2 6.5 slice.624
  566.7 11.2 slice.527
  577.9 11.6 slice.622
  589.5 11.2 slice.626
  600.7 11.2 slice.630
  611.9 20.5 %slice.517 = f32[127,1024]{0,1:T(8,128)} slice(f32[256,1024]{0,1:T(8,128)} %get-tuple-element.229), slice={[2:256:2], [0:1024:1]} | slice | bytes 1040384 | tf_op jit(solution)/shard_map/slice | solution.py:50
  632.4 20.5 %slice.628 = f32[127,1024]{0,1:T(8,128)} slice(f32[256,1024]{0,1:T(8,128)} %get-tuple-element.230), slice={[2:256:2], [0:1024:1]} | slice | bytes 1040384 | tf_op jit(solution)/shard_map/slice | solution.py:50
  653.0 20.7 %slice.632 = f32[127,1024]{0,1:T(8,128)} slice(f32[256,1024]{0,1:T(8,128)} %get-tuple-element.228), slice={[2:256:2], [0:1024:1]} | slice | bytes 1040384 | tf_op jit(solution)/shard_map/slice | solution.py:50
  673.6 20.5 %slice.673 = f32[127,1024]{0,1:T(8,128)} slice(f32[256,1024]{0,1:T(8,128)} %get-tuple-element.227), slice={[2:256:2], [0:1024:1]} | slice | bytes 1040384 | tf_op jit(solution)/shard_map/slice | solution.py:50
  876.6 6.9 pad.218
  883.5 7.1 pad.219
  890.6 7.0 pad.217
  899.8 7.0 pad.216
  914.3 11.2 pad.222
  925.5 11.4 pad.223
  938.9 11.3 pad.220
  950.2 11.3 pad.221
  982.2 21.9 %pad.258 = f32[256,1024]{0,1:T(8,128)} pad(f32[128,1024]{0,1:T(8,128)} %pad_maximum_fusion.15, f32[]{:T(128)} %constant.66.clone.1), padding=0_1_1x0_0_0 | pad | bytes 1572868 | tf_op jit(solution)/shard_map/pad | solution.py:50
  1004.1 20.0 %pad.259 = f32[256,1024]{0,1:T(8,128)} pad(f32[128,1024]{0,1:T(8,128)S(1)} %copy-done.122, f32[]{:T(128)} %constant.66.clone.1), padding=1_0_1x0_0_0 | pad | bytes 1572868 | tf_op jit(solution)/shard_map/pad | solution.py:50
  1027.6 21.8 %pad.225 = f32[256,1024]{0,1:T(8,128)} pad(f32[128,1024]{0,1:T(8,128)} %add.588, f32[]{:T(128)} %constant.66.clone.1), padding=1_0_1x0_0_0 | pad | bytes 1572868 | tf_op jit(solution)/shard_map/pad | solution.py:50
  1051.4 22.0 %pad.224 = f32[256,1024]{0,1:T(8,128)} pad(f32[128,1024]{0,1:T(8,128)} %pad_maximum_fusion.6, f32[]{:T(128)} %constant.66.clone.1), padding=0_1_1x0_0_0 | pad | bytes 1572868 | tf_op jit(solution)/shard_map/pad | solution.py:50
  1133.4 7.0 pad.248
  1140.3 7.0 pad.249
  1147.3 7.0 pad.247
  1156.4 6.9 pad.246
  1168.9 10.3 pad.252
  1179.2 11.3 pad.253
  1192.5 21.8 %pad.257 = f32[256,1024]{0,1:T(8,128)} pad(f32[128,1024]{0,1:T(8,128)} %add.615, f32[]{:T(128)} %constant.66.clone.1), padding=1_0_1x0_0_0 | pad | bytes 1572868 | tf_op jit(solution)/shard_map/pad | solution.py:50
  1216.4 9.8 pad.250
  1226.2 11.4 pad.251
  1244.4 19.9 %pad.256 = f32[256,1024]{0,1:T(8,128)} pad(f32[128,1024]{0,1:T(8,128)S(1)} %pad_maximum_fusion.14, f32[]{:T(128)} %constant.66.clone.1), padding=0_1_1x0_0_0 | pad | bytes 1572868 | tf_op jit(solution)/shard_map/pad | solution.py:50
  1268.0 20.0 %pad.255 = f32[256,1024]{0,1:T(8,128)} pad(f32[128,1024]{0,1:T(8,128)S(1)} %copy-done.123, f32[]{:T(128)} %constant.66.clone.1), padding=1_0_1x0_0_0 | pad | bytes 1572868 | tf_op jit(solution)/shard_map/pad | solution.py:50
  1289.4 20.0 %pad.254 = f32[256,1024]{0,1:T(8,128)} pad(f32[128,1024]{0,1:T(8,128)S(1)} %pad_maximum_fusion.13, f32[]{:T(128)} %constant.66.clone.1), padding=0_1_1x0_0_0 | pad | bytes 1572868 | tf_op jit(solution)/shard_map/pad | solution.py:50
  1313.0 31.0 %all_gather.24 = f32[8,16,64]{2,1,0:T(8,128)S(1)} all-gather(f32[1,16,64]{2,1,0:T(8,128)S(1)} %slice.675), channel_id=1, replica_groups=mesh['ep'=8,'tp'=4] {'ep'}, dimensions={0}, use_global_device_ids=true | all-gather | bytes 36864 | tf_op jit(solution)/shard_map/all_gather | solution.py:11
  1344.1 30.5 %all_gather.23 = f32[8,16,64]{2,1,0:T(8,128)S(1)} all-gather(f32[1,16,64]{2,1,0:T(8,128)S(1)} %slice.670), channel_id=1, replica_groups=mesh['ep'=8,'tp'=4] {'ep'}, dimensions={0}, use_global_device_ids=true | all-gather | bytes 36864 | tf_op jit(solution)/shard_map/all_gather | solution.py:11
  1374.6 30.5 %all_gather.22 = f32[8,16,64]{2,1,0:T(8,128)S(1)} all-gather(f32[1,16,64]{2,1,0:T(8,128)S(1)} %slice.668), channel_id=1, replica_groups=mesh['ep'=8,'tp'=4] {'ep'}, dimensions={0}, use_global_device_ids=true | all-gather | bytes 36864 | tf_op jit(solution)/shard_map/all_gather | solution.py:11
  1405.1 30.6 %all_gather.21 = f32[8,16,64]{2,1,0:T(8,128)S(1)} all-gather(f32[1,16,64]{2,1,0:T(8,128)S(1)} %slice.664), channel_id=1, replica_groups=mesh['ep'=8,'tp'=4] {'ep'}, dimensions={0}, use_global_device_ids=true | all-gather | bytes 36864 | tf_op jit(solution)/shard_map/all_gather | solution.py:11
  1451.8 7.4 all_gather.25
  1462.0 7.3 all_gather.26
  (572 shorter events, 571.9 us)
Async XLA Ops:
  7.2 958.3 %copy-start = (bf16[1,2048,512]{2,1,0:T(8,128)(2,1)S(1)}, bf16[1,2048,512]{2,1,0:T(8,128)(2,1)}, u32[]{:S(2)}) copy-start(bf16[1,2048,512]{2,1,0:T(8,128)(2,1)} %param.37) | copy-start | bytes 6291460
  28.7 7.5 copy-start.126
  28.7 7.6 copy-start.128
  28.7 936.7 %all-to-all-start = ((bf16[8,128,2048]{2,1,0:T(8,128)(2,1)}), bf16[8,128,2048]{2,1,0:T(8,128)(2,1)}, u32[]{:S(2)}, u32[]{:S(2)}) async-start(bf16[8,128,2048]{2,1,0:T(8,128)(2,1)} %broadcast_select_fusion), calls=%async_computation | async-start | bytes 8388608 | tf_op jit(solution)/shard_map/all_to_all | solution.py:163
  36.2 1403.4 %all-gather.2.cloned.1.call-start = ((), (), s32[]{:S(2)}) async-start(), calls=%async_computation.2 | async-start | bytes 5242880 | tf_op jit(solution)/shard_map/all_gather | solution.py:174
  217.1 44.7 %copy-start.2 = (f32[128,1024]{0,1:T(8,128)}, f32[128,1024]{0,1:T(8,128)S(1)}, u32[]{:S(2)}) copy-start(f32[128,1024]{0,1:T(8,128)S(1)} %get-tuple-element.179) | copy-start | bytes 1572868
  261.8 22.6 %copy-start.14 = (f32[128,1024]{0,1:T(8,128)S(1)}, f32[128,1024]{0,1:T(8,128)}, u32[]{:S(2)}) copy-start(f32[128,1024]{0,1:T(8,128)} %get-tuple-element.128) | copy-start | bytes 1572868
  309.8 25.0 %copy-start.5 = (f32[64,1024]{0,1:T(8,128)}, f32[64,1024]{0,1:T(8,128)S(1)}, u32[]{:S(2)}) copy-start(f32[64,1024]{0,1:T(8,128)S(1)} %get-tuple-element.177) | copy-start | bytes 786436
  334.8 13.2 copy-start.17
  363.2 17.1 %copy-start.8 = (f32[32,1024]{0,1:T(8,128)}, f32[32,1024]{0,1:T(8,128)S(1)}, u32[]{:S(2)}) copy-start(f32[32,1024]{0,1:T(8,128)S(1)} %get-tuple-element.175) | copy-start | bytes 393220
  380.4 9.9 copy-start.20
  400.9 14.3 copy-start.11
  415.2 8.7 copy-start.23
  433.1 12.9 copy-start.24
  446.0 7.8 copy-start.26
  706.7 6.1 copy-start.28
  713.9 9.6 copy-start.121
  723.7 6.5 copy-start.125
  735.0 9.1 copy-start.30
  746.8 8.8 copy-start.45
  755.6 5.1 copy-start.55
  755.6 5.1 copy-start.60
  763.8 8.5 copy-start.27
  772.5 9.5 copy-start.25
  807.4 4.4 copy-start.52
  807.4 5.3 copy-start.59
  807.4 5.3 copy-start.61
  817.0 8.5 copy-start.22
  846.6 10.8 copy-start.19
  859.4 9.8 copy-start.62
  875.6 22.1 %copy-start.16 = (f32[64,1024]{0,1:T(8,128)S(1)}, f32[64,1024]{0,1:T(8,128)}, u32[]{:S(2)}) copy-start(f32[64,1024]{0,1:T(8,128)} %get-tuple-element.127) | copy-start | bytes 786436
  899.8 11.3 copy-start.63
  906.7 4.3 copy-start.65
  906.7 4.3 copy-start.66
  906.7 4.3 copy-start.72
  906.7 4.3 copy-start.77
  906.7 4.3 copy-start.79
  906.7 4.3 copy-start.114
  913.3 23.6 %copy-start.13 = (f32[128,1024]{0,1:T(8,128)S(1)}, f32[128,1024]{0,1:T(8,128)}, u32[]{:S(2)}) copy-start(f32[128,1024]{0,1:T(8,128)} %get-tuple-element.129) | copy-start | bytes 1572868
  938.9 22.6 %copy-start.43 = (f32[128,1024]{0,1:T(8,128)S(1)}, f32[128,1024]{0,1:T(8,128)}, u32[]{:S(2)}) copy-start(f32[128,1024]{0,1:T(8,128)} %pad.222) | copy-start | bytes 1572868
  965.5 4.7 copy-start.135
  981.2 22.9 %copy-start.122 = (f32[128,1024]{0,1:T(8,128)S(1)}, f32[128,1024]{0,1:T(8,128)}, u32[]{:S(2)}) copy-start(f32[128,1024]{0,1:T(8,128)} %add.591) | copy-start | bytes 1572868
  1027.0 22.4 %copy-start.111 = (f32[1,16,64]{0,2,1:T(8,128)S(1)}, f32[1,16,64]{0,2,1:T(8,128)}, u32[]{:S(2)}) copy-start(f32[1,16,64]{0,2,1:T(8,128)} %get-tuple-element.145) | copy-start | bytes 12292
  1076.3 7.8 copy-start.12
  1084.2 8.5 copy-start.124
  1095.5 8.0 copy-start.86
  1104.6 10.6 copy-start.9
  1122.1 9.2 copy-start.82
  1132.4 22.0 %copy-start.6 = (f32[64,1024]{0,1:T(8,128)S(1)}, f32[64,1024]{0,1:T(8,128)}, u32[]{:S(2)}) copy-start(f32[64,1024]{0,1:T(8,128)} %copy-done.5) | copy-start | bytes 786436
  1156.4 11.2 copy-start.78
  1163.3 4.3 copy-start.99
  1163.3 4.3 copy-start.107
  1179.2 35.1 %copy-start.3 = (f32[128,1024]{0,1:T(8,128)S(1)}, f32[128,1024]{0,1:T(8,128)}, u32[]{:S(2)}) copy-start(f32[128,1024]{0,1:T(8,128)} %copy-done.2) | copy-start | bytes 1572868
  1237.6 5.7 copy-start.74
  1237.6 5.7 copy-start.76
  1237.6 5.7 copy-start.93
  1237.6 5.7 copy-start.94
  1237.6 5.7 copy-start.100
  1309.4 126.3 %copy-start.127 = (bf16[2,16,16,64]{3,2,1,0:T(8,128)(2,1)S(1)}, bf16[2,16,16,64]{3,2,1,0:T(8,128)(2,1)}, u32[]{:S(2)}) copy-start(bf16[2,16,16,64]{3,2,1,0:T(8,128)(2,1)} %param.28) | copy-start | bytes 196612
  1445.7 6.0 copy-start.134
  1445.7 24.8 %all-to-all-start.1 = ((bf16[8,128,512]{2,1,0:T(8,128)(2,1)}), bf16[8,128,512]{2,1,0:T(8,128)(2,1)}, u32[]{:S(2)}, u32[]{:S(2)}) async-start(bf16[8,128,512]{2,1,0:T(8,128)(2,1)} %bitcast.204), calls=%async_computation.1 | async-start | bytes 2097152 | tf_op jit(solution)/shard_map/all_to_all | solution.py:184
  1451.8 9.7 copy-start.136
  1461.5 7.8 copy-start.137
  1461.5 7.8 copy-start.138
  (78 other events, 249.3 us)
Sparse Core Ops, SparseCore 0:
  976.2 35.8 all-gather.1
where the time goes:
time: 1500 us; the launch traced here: 1490 us
  local copies, waits for them, and re-layouts  1130 us (75%)
  other arithmetic  162 us (11%)
  blocking collectives  137 us (9%)
  matrix products  26.9 us (2%)
  between operations  15.7 us (1%)
    slice x81, local copies, waits for them, and re-layouts, local_states(): scanned = lax.associative_scan(combine_steps, flat_operands, axis=0)  626 us
    pad x56, local copies, waits for them, and re-layouts, local_states(): scanned = lax.associative_scan(combine_steps, flat_operands, axis=0)  424 us
    all_gather x4, blocking collectives, entering(): gathered = jax.tree.map(lambda a: lax.all_gather(a, axis), part)  123 us
    add x30, other arithmetic, local_states(): scanned = lax.associative_scan(combine_steps, flat_operands, axis=0)  62.3 us
    add x15, other arithmetic, combine_steps(): latter[0] * earlier[3] + latter[1] * earlier[2] + latter[3]  32.6 us
  transfers between devices with their start and end apart: 3, of which 0 were waited for; matrix products, arithmetic and copies ran while one was open for 86% of the time, Pallas kernels for 0%

commit v1 on v0

v1 whole, which is shorter than its diff:
```python
import jax
import jax.numpy as jnp
from jax import lax
from jax.experimental import pallas as pl
from jax.experimental.pallas import tpu as pltpu
from jax.sharding import PartitionSpec as P

eps_norm = 1e-06
LANES = 128
ROWS = 8


def cos_sin(angle):
    turns = jnp.floor(angle * 0.6366197723675814 + 0.5)
    rest = ((angle - turns * 1.5703125) - turns * 4.837512969970703125e-4) - turns * 7.549789954891882e-8
    square = rest * rest
    sine = rest + rest * square * (
        -1.6666654611e-1 + square * (8.3321608736e-3 + square * -1.9515295891e-4)
    )
    cosine = (
        1.0
        - 0.5 * square
        + square
        * square
        * (
            4.166664568298827e-2
            + square * (-1.388731625493765e-3 + square * 2.443315711809948e-5)
        )
    )
    quarter = turns.astype(jnp.int32)
    odd = (quarter & 1) == 1
    out_cos = jnp.where(odd, sine, cosine)
    out_sin = jnp.where(odd, cosine, sine)
    out_cos = jnp.where(((quarter + 1) & 2) == 2, -out_cos, out_cos)
    out_sin = jnp.where((quarter & 2) == 2, -out_sin, out_sin)
    return out_cos, out_sin


def one_minus_exp_neg(y):
    series = y * (
        1.0
        - y / 2
        * (1.0 - y / 3 * (1.0 - y / 4 * (1.0 - y / 5 * (1.0 - y / 6))))
    )
    return jnp.where(y < 0.3, series, 1.0 - jnp.exp(-y))


def scan_kernel(
    u_ref, win_ref, step_ref, loss_ref, eig_ref, freq_ref,
    reach_r_ref, reach_i_ref, state_r_ref, state_i_ref, ends_ref,
    ar_ref, ai_ref, br_ref, bi_ref,
):
    rows = u_ref.shape[0]
    u = u_ref[...]
    lane = lax.broadcasted_iota(jnp.int32, (rows, LANES), 1)
    half = lane < (LANES // step_ref.shape[2])
    step = jnp.where(half, step_ref[0, :, 0:1], step_ref[0, :, 1:2])
    loss = jnp.where(half, loss_ref[0, :, 0:1], loss_ref[0, :, 1:2])
    loss_rate = eig_ref[0] * step
    magnitude = jnp.exp(loss - loss_rate)
    cosine, sine = cos_sin(freq_ref[0] * step)
    scaling = jnp.sqrt(one_minus_exp_neg(2.0 * loss_rate))
    ar_ref[...] = magnitude * cosine
    ai_ref[...] = magnitude * sine
    br_ref[...] = scaling * jnp.dot(u, win_ref[0], preferred_element_type=jnp.float32)
    bi_ref[...] = scaling * jnp.dot(u, win_ref[1], preferred_element_type=jnp.float32)
    count = rows // ROWS
    reach = jnp.ones((ROWS, LANES), jnp.float32), jnp.zeros((ROWS, LANES), jnp.float32)
    state = jnp.zeros((ROWS, LANES), jnp.float32), jnp.zeros((ROWS, LANES), jnp.float32)
    for j in range(count):
        at = pl.ds(j * ROWS, ROWS)
        ar, ai, br, bi = ar_ref[at, :], ai_ref[at, :], br_ref[at, :], bi_ref[at, :]
        reach = ar * reach[0] - ai * reach[1], ar * reach[1] + ai * reach[0]
        state = ar * state[0] - ai * state[1] + br, ar * state[1] + ai * state[0] + bi
        ar_ref[at, :] = reach[0]
        ai_ref[at, :] = reach[1]
        br_ref[at, :] = state[0]
        bi_ref[at, :] = state[1]
    row = lax.broadcasted_iota(jnp.int32, (ROWS, LANES), 0)
    er, ei = jnp.ones((1, LANES), jnp.float32), jnp.zeros((1, LANES), jnp.float32)
    sr, si = jnp.zeros((1, LANES), jnp.float32), jnp.zeros((1, LANES), jnp.float32)
    pre_r, pre_i = reach[0] * 0.0, reach[0] * 0.0
    pre_sr, pre_si = pre_r, pre_r
    for s in range(ROWS):
        here = row == s
        pre_r = jnp.where(here, er, pre_r)
        pre_i = jnp.where(here, ei, pre_i)
        pre_sr = jnp.where(here, sr, pre_sr)
        pre_si = jnp.where(here, si, pre_si)
        tr, ti = reach[0][s : s + 1], reach[1][s : s + 1]
        ur, ui = state[0][s : s + 1], state[1][s : s + 1]
        er, ei, sr, si = (
            tr * er - ti * ei,
            tr * ei + ti * er,
            tr * sr - ti * si + ur,
            tr * si + ti * sr + ui,
        )
    for j in range(count):
        at = pl.ds(j * ROWS, ROWS)
        ar, ai = ar_ref[at, :], ai_ref[at, :]
        state_r_ref[at, :] = br_ref[at, :] + ar * pre_sr - ai * pre_si
        state_i_ref[at, :] = bi_ref[at, :] + ar * pre_si + ai * pre_sr
        reach_r_ref[at, :] = ar * pre_r - ai * pre_i
        reach_i_ref[at, :] = ar * pre_i + ai * pre_r
    ends_ref[0, 0:1] = er
    ends_ref[0, 1:2] = ei
    ends_ref[0, 2:3] = sr
    ends_ref[0, 3:4] = si


def read_kernel(
    hops, ends_ref, reach_r_ref, reach_i_ref, state_r_ref, state_i_ref, wout_ref, u_ref, feed_ref,
    out_ref, total_ref,
):
    tile = pl.program_id(0)
    place = jnp.full((1, LANES), lax.axis_index("ep"), jnp.int32)
    sr, si = jnp.zeros((1, LANES), jnp.float32), jnp.zeros((1, LANES), jnp.float32)
    for hop in range(hops - 1):
        keep = place > hop
        tr, ti = ends_ref[hop, 0, 0:1], ends_ref[hop, 0, 1:2]
        ur, ui = ends_ref[hop, 0, 2:3], ends_ref[hop, 0, 3:4]
        sr, si = (
            jnp.where(keep, tr * sr - ti * si + ur, sr),
            jnp.where(keep, tr * si + ti * sr + ui, si),
        )
    reach_r, reach_i = reach_r_ref[...], reach_i_ref[...]
    state_r = state_r_ref[...] + reach_r * sr - reach_i * si
    state_i = state_i_ref[...] + reach_r * si + reach_i * sr

    def product(state, weight):
        high = state.astype(jnp.bfloat16)
        low = (state - high.astype(jnp.float32)).astype(jnp.bfloat16)
        return jnp.dot(high, weight, preferred_element_type=jnp.float32) + jnp.dot(
            low, weight, preferred_element_type=jnp.float32
        )

    part = product(state_r, wout_ref[0]) - product(state_i, wout_ref[1])

    @pl.when(tile == 0)
    def _():
        total_ref[...] = part + feed_ref[...] * u_ref[...].astype(jnp.float32)

    @pl.when(tile > 0)
    def _():
        total_ref[...] += part

    @pl.when(tile == pl.num_programs(0) - 1)
    def _():
        value = total_ref[...]
        inner = 0.7978845608028654 * (value + 0.044715 * (value * value * value))
        out_ref[...] = (0.5 * value * (1.0 + jnp.tanh(inner))).astype(out_ref.dtype)


def mixer_local(
    inputs, step_logs, losses, eigen, frequency, group_in, group_out, feedthrough
):
    positions, channels = inputs.shape
    groups, states = eigen.shape
    width = groups * states
    tiles = width // LANES
    per_tile = groups // tiles
    seg = positions // ROWS

    def shuffled(rows):
        return rows.reshape(ROWS, seg, -1).transpose(1, 0, 2).reshape(positions, -1)

    def by_tile(table):
        wide = shuffled(table.T).reshape(positions, tiles, per_tile)
        return wide.transpose(1, 0, 2)

    u = shuffled(inputs)
    same = jnp.eye(groups, dtype=bool)
    zero = jnp.zeros((), group_in.dtype)
    win = jnp.where(
        same[None, :, None, :, None], group_in.transpose(0, 1, 3, 2)[:, :, :, None, :], zero
    ).reshape(2, channels, width)
    wout = jnp.where(
        same[None, :, None, :, None], group_out.transpose(0, 1, 3, 2)[:, :, :, None, :], zero
    ).reshape(2, width, channels)
    column = pl.BlockSpec((positions, LANES), lambda i: (0, i))
    whole_u = pl.BlockSpec((positions, channels), lambda i: (0, 0))
    pair = pl.BlockSpec((1, positions, per_tile), lambda i: (i, 0, 0))
    lane_row = pl.BlockSpec((1, 1, LANES), lambda i: (i, 0, 0))
    wide_shape = jax.ShapeDtypeStruct((positions, width), jnp.float32)
    column_scratch = pltpu.VMEM((positions, LANES), jnp.float32)
    reach_r, reach_i, state_r, state_i, ends = pl.pallas_call(
        scan_kernel,
        grid=(tiles,),
        in_specs=[
            whole_u,
            pl.BlockSpec((2, channels, LANES), lambda i: (0, 0, i)),
            pair,
            pair,
            lane_row,
            lane_row,
        ],
        out_specs=[column, column, column, column, pl.BlockSpec((1, 4, LANES), lambda i: (i, 0, 0))],
        out_shape=[wide_shape] * 4 + [jax.ShapeDtypeStruct((tiles, 4, LANES), jnp.float32)],
        scratch_shapes=[column_scratch] * 4,
        cost_estimate=pl.CostEstimate(
            flops=positions * channels * width * 4, bytes_accessed=24 * positions * width,
            transcendentals=4 * positions * width,
        ),
        name="scan_states",
    )(
        u,
        win,
        by_tile(jnp.exp(step_logs)),
        by_tile(losses),
        eigen.reshape(tiles, 1, LANES),
        frequency.reshape(tiles, 1, LANES),
    )
    hops = lax.axis_size("ep")
    all_ends = lax.all_gather(ends, "ep")
    out = pl.pallas_call(
        lambda *refs: read_kernel(hops, *refs),
        grid=(tiles,),
        in_specs=[
            pl.BlockSpec((hops, 1, 4, LANES), lambda i: (0, i, 0, 0)),
            column, column, column, column,
            pl.BlockSpec((2, LANES, channels), lambda i: (0, i, 0)),
            whole_u,
            pl.BlockSpec((1, channels), lambda i: (0, 0)),
        ],
        out_specs=whole_u,
        out_shape=jax.ShapeDtypeStruct((positions, channels), jnp.bfloat16),
        scratch_shapes=[pltpu.VMEM((positions, channels), jnp.float32)],
        cost_estimate=pl.CostEstimate(
            flops=positions * channels * width * 8, bytes_accessed=24 * positions * width,
            transcendentals=positions * channels,
        ),
        name="read_states",
    )(all_ends, reach_r, reach_i, state_r, state_i, wout, u, feedthrough.reshape(1, channels))
    return out.reshape(seg, ROWS, channels).transpose(1, 0, 2).reshape(positions, channels)


def scaled_rows(values, gain):
    widened = values.astype(jnp.float32)
    factor = lax.rsqrt(jnp.mean(widened * widened, axis=-1, keepdims=True) + eps_norm)
    return (widened * factor * gain).astype(jnp.bfloat16)


def gated(rows, gate_weight, up_weight):
    gate_part = jnp.dot(rows, gate_weight, preferred_element_type=jnp.float32)
    up_part = jnp.dot(rows, up_weight, preferred_element_type=jnp.float32)
    return (jax.nn.silu(gate_part) * up_part).astype(jnp.bfloat16)


def on_device(
    mixer_group_input,
    log_step_size,
    extra_log_decay,
    negated_eigen_real,
    frequency,
    group_input_matrices,
    group_output_matrices,
    channel_feedthrough,
    mixer_norm_scale,
    mixer_output_weight,
    second_micro_input,
    expert_norm_scale,
    routes,
    chosen_expert_weight,
    expert_gate_weight,
    expert_up_weight,
    expert_down_weight,
    shared_gate_weight,
    shared_up_weight,
    shared_down_weight,
):
    token_count, top_count = routes.shape
    experts = lax.axis_size("ep")
    column_count = expert_down_weight.shape[2]
    gate_weight, up_weight, down_weight = (
        expert_gate_weight[0],
        expert_up_weight[0],
        expert_down_weight[0],
    )
    normed_tokens = scaled_rows(second_micro_input, expert_norm_scale)
    all_tokens = lax.all_gather(normed_tokens, "ep", axis=0, tiled=True)
    ssm_out = mixer_local(
        mixer_group_input,
        log_step_size,
        extra_log_decay,
        negated_eigen_real,
        frequency,
        group_input_matrices,
        group_output_matrices,
        channel_feedthrough,
    )
    shared_hidden = gated(normed_tokens, shared_gate_weight, shared_up_weight)
    whole_rows = lax.all_gather(ssm_out, "tp", axis=1, tiled=True)
    whole_shared = lax.all_gather(shared_hidden, "tp", axis=1, tiled=True)
    hidden = gated(all_tokens, gate_weight, up_weight)
    whole_hidden = lax.all_gather(hidden, "tp", axis=1, tiled=True)
    normed_mix = scaled_rows(whole_rows, mixer_norm_scale)
    mixed = jnp.dot(normed_mix, mixer_output_weight, preferred_element_type=jnp.float32).astype(
        jnp.bfloat16
    )
    shared_columns = jnp.dot(
        whole_shared, shared_down_weight, preferred_element_type=jnp.float32
    )
    results = (
        jnp.dot(whole_hidden, down_weight, preferred_element_type=jnp.float32)
        .astype(jnp.bfloat16)
        .reshape(experts, token_count, column_count)
    )
    returned = lax.all_to_all(results, "ep", split_axis=0, concat_axis=0, tiled=True)
    share = jnp.sum(
        jnp.where(
            routes[:, :, None] == jnp.arange(experts, dtype=jnp.int32),
            chosen_expert_weight[:, :, None],
            0.0,
        ),
        axis=1,
    )
    combined = jnp.sum(returned.astype(jnp.float32) * share.T[:, :, None], axis=0)
    moe_out = (shared_columns + combined).astype(jnp.bfloat16)
    return (mixed, moe_out)


def solution(mesh):
    return jax.shard_map(
        on_device,
        mesh=mesh,
        in_specs=(
            P("ep", "tp"),
            P("tp", "ep"),
            P("tp", "ep"),
            P("tp", None),
            P("tp", None),
            P(None, "tp", None, None),
            P(None, "tp", None, None),
            P("tp"),
            P(),
            P(None, "tp"),
            P("ep", None),
            P(),
            P("ep", None),
            P("ep", None),
            P("ep", None, "tp"),
            P("ep", None, "tp"),
            P("ep", None, "tp"),
            P(None, "tp"),
            P(None, "tp"),
            P(None, "tp"),
        ),
        out_specs=(P("ep", "tp"), P("ep", "tp")),
        check_vma=False,
    )
```

time: 1500 us -> 235 us (0.16)
  local copies, waits for them, and re-layouts: 1130 us -> 33.1 us
  other arithmetic: 162 us -> 7.54 us
  waiting for transfers between devices: 0.04 us -> 75.7 us
  blocking collectives: 137 us -> 61.4 us
  Pallas kernels: 0 us -> 16.7 us
    slice x86 -> x0, local copies, waits for them, and re-layouts: 627 us -> none  [the longest x81 626 us: local_states(): scanned = lax.associative_scan(combine_steps, flat_operands, axis=0)]
    pad x56 -> x0, local copies, waits for them, and re-layouts: 424 us -> none  [local_states(): scanned = lax.associative_scan(combine_steps, flat_operands, axis=0)]
    add x54 -> x0, other arithmetic: 98.1 us -> none  [the longest x30 62.3 us: local_states(): scanned = lax.associative_scan(combine_steps, flat_operands, axis=0)]
    all_gather x5 -> x2, blocking collectives: 130 us -> 54.1 us  [the longest x1 46.8 us: mixer_local(): all_ends = lax.all_gather(ends, 'ep')]
    all_gather x1 -> x2, waiting for transfers between devices: 0.02 us -> 75.6 us  [the longest x1 75.6 us: on_device(): all_tokens = lax.all_gather(normed_tokens, 'ep', axis=0, tiled=True)]
    mul x28 -> x0, local copies, waits for them, and re-layouts: 29.1 us -> none  [the longest x3 3.79 us: combine_steps(): earlier[0] * latter[1] + earlier[1] * latter[0]]
    mul x8 -> x0, other arithmetic: 25.5 us -> none  [the longest x2 9.61 us: local_states(): scaling * driven[1]]
    concatenate x28 -> x0, other arithmetic: 22.4 us -> none  [local_states(): scanned = lax.associative_scan(combine_steps, flat_operands, axis=0)]
  transfers between devices with their start and end apart: 3 -> 3, of which waited for: 0 -> 1; matrix products, arithmetic and copies ran while one was open for 86% -> 17% of each run, Pallas kernels for 0% -> 7%
where the time goes in v1:
time: 235 us; the launch traced here: 234 us
  waiting for transfers between devices  75.7 us (32%)
  blocking collectives  61.4 us (26%)
  local copies, waits for them, and re-layouts  33.1 us (14%)
  matrix products  21 us (9%)
  Pallas kernels  16.7 us (7%)
  between operations  14.3 us (6%)
  other arithmetic  7.54 us (3%)
  starting transfers between devices  4.45 us (2%)
    all_gather x1, waiting for transfers between devices, on_device(): all_tokens = lax.all_gather(normed_tokens, 'ep', axis=0, tiled=True)  75.6 us
    all_gather x1, blocking collectives, mixer_local(): all_ends = lax.all_gather(ends, 'ep')  46.8 us
    broadcast_in_dim x6, local copies, waits for them, and re-layouts, mixer_local(): jnp.where(same[None, :, None, :, None], group_out.transpose(0, 1, 3, 2)[:...  14.3 us
    pallas_call x1, Pallas kernels, mixer_local(): pl.pallas_call(scan_kernel, grid=(tiles,), in_specs=[whole_u, pl.BlockSpe...  9.23 us
    pallas_call x1, Pallas kernels, mixer_local(): pl.pallas_call(lambda *refs: read_kernel(hops, *refs), grid=(tiles,), in_...  7.46 us
    all_gather x1, blocking collectives, on_device(): whole_rows = lax.all_gather(ssm_out, 'tp', axis=1, tiled=True)  7.3 us
    all_gather x1, blocking collectives, on_device(): whole_shared = lax.all_gather(shared_hidden, 'tp', axis=1, tiled=True)  7.28 us
    dot_general x1, matrix products, on_device(): jnp.dot(whole_hidden, down_weight, preferred_element_type=jnp.float32)  6.22 us
  transfers between devices with their start and end apart: 3, of which 1 were waited for; matrix products, arithmetic and copies ran while one was open for 17% of the time, Pallas kernels for 7%

profile of v1, /device:TPU:0, one launch (start us, length us, event | category | flops | bytes accessed | tf_op | source)
XLA Modules:
  0.0 234.1 jit_solution(252957274547700532)
XLA Ops:
  7.2 0.0 copy-start
  7.2 0.0 all-gather.4.cloned.1.call-start
  7.2 1.4 fusion.16
  8.6 2.0 fusion.18
  10.7 0.0 all-gather.4.cloned.1.call-update
  10.7 0.0 all-gather.6.cloned.1.call-start
  10.7 75.6 %all-gather.4.cloned.1.call-done = bf16[1024,2048]{1,0:T(8,128)(2,1)} async-done(((bf16[128,2048]{1,0:T(8,128)(2,1)}), bf16[1024,2048]{1,0:T(8,128)(2,1)}) %all-gather.4.cloned.1.call-update) | async-done | bytes 4194320 | tf_op jit(solution)/shard_map/all_gather | solution.py:280
  86.3 0.0 copy-done
  86.3 4.7 %fusion.2 = f32[1024,512]{1,0:T(8,128)S(1)} fusion(bf16[1024,2048]{1,0:T(8,128)(2,1)} %all-gather.4.cloned.1.call-done, bf16[1,2048,512]{2,1,0:T(8,128)(2,1)S(1)} %copy-done), kind=kOutput, calls=%fused_computation.2 | convolution fusion | flops 2147483648 | bytes 8388608 | tf_op jit(solution)/shard_map/dot_general | solution.py:245
  91.0 0.0 copy-done.12
  91.0 0.0 copy-done.13
  91.0 3.7 %multiply_convert_fusion = bf16[1024,512]{1,0:T(8,128)(2,1)} fusion(f32[1024,512]{1,0:T(8,128)S(1)} %fusion.2, bf16[1024,2048]{1,0:T(8,128)(2,1)S(1)} %copy-done.12, bf16[1,2048,512]{2,1,0:T(8,128)(2,1)S(1)} %copy-done.13), kind=kOutput, calls=%fused_computation.7 | convolution fusion | flops 2150629376 | bytes 9437184 | tf_op jit(solution)/shard_map/dot_general | solution.py:244
  94.7 0.0 all-gather.6.cloned.1.call-update
  94.7 0.0 copy-start.7
  94.8 0.6 copy-done.7
  95.3 0.1 copy.51
  95.4 0.2 broadcast_in_dim.76
  95.6 0.8 broadcast_in_dim.77
  96.4 0.0 copy-done.4
  96.4 1.7 broadcast_in_dim.79
  98.1 3.4 %broadcast_in_dim.80 = bf16[2,256,1024]{2,1,0:T(8,128)(2,1)S(1)} reshape(bf16[2,16,16,16,64]{4,3,2,1,0:T(8,128)(2,1)} %broadcast_in_dim.79) | data formatting | bytes 2097152 | tf_op jit(solution)/shard_map/jit(_where)/broadcast_in_dim | solution.py:174
  101.5 0.0 copy-done.5
  101.5 0.7 copy.61
  102.2 0.7 exponential_bitcast_fusion
  102.9 0.1 reshape.72
  103.0 0.8 copy.52
  103.9 1.1 reshape_reshape.6
  105.0 1.4 copy.53
  106.3 0.0 copy-done.8
  106.4 0.1 reshape.73
  106.4 0.8 copy.54
  107.3 1.2 reshape_reshape.7
  108.4 1.4 copy.55
  109.9 1.4 reshape.74.eig_ref
  111.2 1.4 reshape.75.freq_ref
  112.6 1.7 broadcast_in_dim.82
  114.3 2.5 %broadcast_in_dim.83 = pred[1024,256]{0,1:T(8,128)(4,1)} reshape(pred[16,64,16,16]{1,0,3,2:T(8,128)(4,1)} %broadcast_in_dim.82) | data formatting | bytes 524288 | tf_op jit(solution)/shard_map/jit(_where)/broadcast_in_dim | solution.py:177
  116.7 2.0 copy.56
  118.7 0.0 copy-done.6
  118.8 1.8 broadcast_in_dim.85
  120.6 4.1 %broadcast_in_dim.86 = bf16[2,1024,256]{1,2,0:T(8,128)(2,1)} reshape(bf16[2,16,64,16,16]{2,1,4,3,0:T(8,128)(2,1)} %broadcast_in_dim.85) | data formatting | bytes 2097152 | tf_op jit(solution)/shard_map/jit(_where)/broadcast_in_dim | solution.py:177
  124.7 2.3 copy.58
  127.0 1.2 broadcast_select_fusion.1.win_ref
  128.2 9.2 %scan_states.1 = (f32[256,1024]{1,0:T(8,128)}, f32[256,1024]{1,0:T(8,128)}, f32[256,1024]{1,0:T(8,128)}, f32[256,1024]{1,0:T(8,128)}, f32[8,4,128]{2,1,0:T(4,128)}) custom-call(bf16[256,256]{1,0:T(8,128)(2,1)} %bitcast.68, bf16[2,256,1024]{2,1,0:T(8,128)(2,1)} %broadcast_select_fusion.1.win_ref, f32[8,256,2]{2,1,0:T(8,128)} %bitcast.66, ...), custom_call_target="tpu_custom_call" | custom-call | flops 268435456 | bytes 6291456 | tf_op jit(solution)/shard_map/scan_states/pallas_call | solution.py:186
  137.4 1.2 broadcast_select_fusion.refs_5_
  138.6 6.2 %fusion.8 = bf16[1024,512]{1,0:T(8,128)(2,1)} fusion(bf16[1024,2048]{1,0:T(8,128)(2,1)} %all-gather.6.cloned.1.call-done, bf16[1,2048,512]{2,1,0:T(8,128)(2,1)} %param.36), kind=kOutput, calls=%fused_computation.8 | convolution fusion | flops 2148007936 | bytes 7340032 | tf_op jit(solution)/shard_map/dot_general | solution.py:304
  144.8 4.4 %all-to-all-start = ((bf16[8,128,512]{2,1,0:T(8,128)(2,1)}), bf16[8,128,512]{2,1,0:T(8,128)(2,1)}, u32[]{:S(2)}, u32[]{:S(2)}) async-start(bf16[8,128,512]{2,1,0:T(8,128)(2,1)} %bitcast.19), calls=%async_computation | async-start | bytes 2097152 | tf_op jit(solution)/shard_map/all_to_all | solution.py:308
  149.2 46.8 %all-gather = f32[64,4,128]{2,1,0:T(4,128)} all-gather(f32[8,4,128]{2,1,0:T(4,128)S(1)} %copy-done.9), channel_id=2, replica_groups=mesh['ep'=8,'tp'=4] {'ep'}, dimensions={0}, use_global_device_ids=true | all-gather | bytes 147456 | tf_op jit(solution)/shard_map/all_gather | solution.py:214
  196.0 7.5 %read_states.1 = bf16[256,256]{1,0:T(8,128)(2,1)} custom-call(f32[8,8,4,128]{3,2,1,0:T(4,128)} %bitcast.72, f32[256,1024]{1,0:T(8,128)} %get-tuple-element.8.refs_1_, f32[256,1024]{1,0:T(8,128)} %get-tuple-element.9.refs_2_, f32[256,1024]{1,0:T(8,128)} %get-tuple-element.10.refs_3_, f32[256,1024]{1,0:T(8,128)} %get-tuple-element.11.refs_4_, ...), custom_call_target="tpu_custom_call" | custom-call | flops 536870912 | bytes 6291456 | tf_op jit(solution)/shard_map/read_states/pallas_call | solution.py:215
  203.5 0.9 copy.59
  204.5 0.0 copy-start.14
  204.5 7.3 %all_gather.20 = bf16[256,1024]{1,0:T(8,128)(2,1)S(1)} all-gather(bf16[256,256]{1,0:T(8,128)(2,1)S(1)} %bitcast.74), channel_id=1, replica_groups=mesh['ep'=8,'tp'=4] {'tp'}, dimensions={1}, use_global_device_ids=true | all-gather | bytes 655360 | tf_op jit(solution)/shard_map/all_gather | solution.py:292
  211.8 0.2 fusion.13
  212.0 0.0 copy-done.1
  212.0 2.0 fusion.22
  214.0 0.0 copy-start.15
  214.0 0.0 copy-start.16
  214.0 0.5 fusion.11
  214.5 7.3 %all_gather.21 = bf16[128,2048]{1,0:T(8,128)(2,1)S(1)} all-gather(bf16[128,512]{1,0:T(8,128)(2,1)S(1)} %fusion.11), channel_id=1, replica_groups=mesh['ep'=8,'tp'=4] {'tp'}, dimensions={1}, use_global_device_ids=true | all-gather | bytes 655360 | tf_op jit(solution)/shard_map/all_gather | solution.py:293
  221.8 0.0 copy-done.15
  221.8 1.2 convolution_convert_fusion
  223.0 0.0 all-to-all-done
  223.0 1.5 multiply_reduce_fusion
  224.5 2.7 %fusion.12 = bf16[128,512]{1,0:T(8,128)(2,1)} fusion(f32[128,512]{1,0:T(8,128)S(1)} %multiply_reduce_fusion, bf16[128,2048]{1,0:T(8,128)(2,1)S(1)} %all_gather.21, bf16[2048,512]{1,0:T(8,128)(2,1)} %param.39), kind=kOutput, calls=%fused_computation.17 | convolution fusion | flops 268566528 | bytes 3014656 | tf_op jit(solution)/shard_map/dot_general | solution.py:300
  (25 shorter events, 0.1 us)
Async XLA Ops:
  7.2 79.2 %copy-start = (bf16[1,2048,512]{2,1,0:T(8,128)(2,1)S(1)}, bf16[1,2048,512]{2,1,0:T(8,128)(2,1)}, u32[]{:S(2)}) copy-start(bf16[1,2048,512]{2,1,0:T(8,128)(2,1)} %param.35) | copy-start | bytes 6291460
  7.2 79.2 %all-gather.4.cloned.1.call-start = ((), (), s32[]{:S(2)}) async-start(), calls=%async_computation.1 | async-start | bytes 4718592 | tf_op jit(solution)/shard_map/all_gather | solution.py:280
  10.7 127.9 %all-gather.6.cloned.1.call-start = ((), (), s32[]{:S(2)}) async-start(), calls=%async_computation.2 | async-start | bytes 5242880 | tf_op jit(solution)/shard_map/all_gather | solution.py:295
  86.3 4.7 %copy-start.12 = (bf16[1024,2048]{1,0:T(8,128)(2,1)S(1)}, bf16[1024,2048]{1,0:T(8,128)(2,1)}, u32[]{:S(2)}) copy-start(bf16[1024,2048]{1,0:T(8,128)(2,1)} %all-gather.4.cloned.1.call-done) | copy-start | bytes 12582916
  86.3 4.7 %copy-start.13 = (bf16[1,2048,512]{2,1,0:T(8,128)(2,1)S(1)}, bf16[1,2048,512]{2,1,0:T(8,128)(2,1)}, u32[]{:S(2)}) copy-start(bf16[1,2048,512]{2,1,0:T(8,128)(2,1)} %param.34) | copy-start | bytes 6291460
  94.7 1.7 copy-start.4
  94.7 0.6 copy-start.7
  98.1 3.4 %copy-start.5 = (bf16[256,256]{1,0:T(8,128)(2,1)S(1)}, bf16[256,256]{1,0:T(8,128)(2,1)}, u32[]{:S(2)}) copy-start(bf16[256,256]{1,0:T(8,128)(2,1)} %param.20) | copy-start | bytes 393220
  98.1 8.3 %copy-start.8 = (f32[16,256]{1,0:T(8,128)S(1)}, f32[16,256]{1,0:T(8,128)}, u32[]{:S(2)}) copy-start(f32[16,256]{1,0:T(8,128)} %param.22) | copy-start | bytes 49156
  107.3 11.5 %copy-start.6 = (bf16[2,16,16,64]{3,2,1,0:T(8,128)(2,1)S(1)}, bf16[2,16,16,64]{3,2,1,0:T(8,128)(2,1)}, u32[]{:S(2)}) copy-start(bf16[2,16,16,64]{3,2,1,0:T(8,128)(2,1)} %param.26) | copy-start | bytes 196612
  128.2 9.2 %copy-start.2 = (bf16[2,1024,256]{2,1,0:T(8,128)(2,1)S(1)}, bf16[2,1024,256]{2,1,0:T(8,128)(2,1)}, u32[]{:S(2)}) copy-start(bf16[2,1024,256]{2,1,0:T(8,128)(2,1)} %copy.58) | copy-start | bytes 3145732
  128.2 9.2 %copy-start.3 = (pred[1024,256]{1,0:T(8,128)(4,1)S(1)}, pred[1024,256]{1,0:T(8,128)(4,1)}, u32[]{:S(2)}) copy-start(pred[1024,256]{1,0:T(8,128)(4,1)} %copy.56) | copy-start | bytes 786436
  144.8 4.4 %copy-start.9 = (f32[8,4,128]{2,1,0:T(4,128)S(1)}, f32[8,4,128]{2,1,0:T(4,128)}, u32[]{:S(2)}) copy-start(f32[8,4,128]{2,1,0:T(4,128)} %get-tuple-element.7) | copy-start | bytes 49156
  144.8 78.2 %all-to-all-start = ((bf16[8,128,512]{2,1,0:T(8,128)(2,1)}), bf16[8,128,512]{2,1,0:T(8,128)(2,1)}, u32[]{:S(2)}, u32[]{:S(2)}) async-start(bf16[8,128,512]{2,1,0:T(8,128)(2,1)} %bitcast.19), calls=%async_computation | async-start | bytes 2097152 | tf_op jit(solution)/shard_map/all_to_all | solution.py:308
  196.0 8.4 %copy-start.10 = (f32[128,4]{0,1:T(4,128)S(1)}, f32[128,4]{0,1:T(4,128)}, u32[]{:S(2)}) copy-start(f32[128,4]{0,1:T(4,128)} %param.33) | copy-start | bytes 6148
  196.0 8.4 %copy-start.11 = (s32[128,4]{0,1:T(4,128)S(1)}, s32[128,4]{0,1:T(4,128)}, u32[]{:S(2)}) copy-start(s32[128,4]{0,1:T(4,128)} %param.32) | copy-start | bytes 6148
  196.0 15.9 %copy-start.1 = (bf16[128,2048]{1,0:T(8,128)(2,1)S(1)}, bf16[128,2048]{1,0:T(8,128)(2,1)}, u32[]{:S(2)}) copy-start(bf16[128,2048]{1,0:T(8,128)(2,1)} %fusion.18) | copy-start | bytes 1572868
  204.5 9.6 %copy-start.14 = (bf16[2048,512]{1,0:T(8,128)(2,1)S(1)}, bf16[2048,512]{1,0:T(8,128)(2,1)}, u32[]{:S(2)}) copy-start(bf16[2048,512]{1,0:T(8,128)(2,1)} %param.38) | copy-start | bytes 6291460
  214.0 7.8 %copy-start.15 = (bf16[1024,512]{1,0:T(8,128)(2,1)S(1)}, bf16[1024,512]{1,0:T(8,128)(2,1)}, u32[]{:S(2)}) copy-start(bf16[1024,512]{1,0:T(8,128)(2,1)} %param.29) | copy-start | bytes 3145732
  214.0 7.8 %copy-start.16 = (f32[1024]{0:T(1024)S(1)}, f32[1024]{0:T(1024)}, u32[]{:S(2)}) copy-start(f32[1024]{0:T(1024)} %param.28) | copy-start | bytes 12292
Sparse Core Ops, SparseCore 0:
  10.8 75.4 all-gather.3
  94.8 33.0 all-gather.5

commit v2 on v1

--- a/solution.py
+++ b/solution.py
@@ -277,7 +277,16 @@
         expert_down_weight[0],
     )
     normed_tokens = scaled_rows(second_micro_input, expert_norm_scale)
-    all_tokens = lax.all_gather(normed_tokens, "ep", axis=0, tiled=True)
+    model_width = normed_tokens.shape[1]
+    part = lax.rem(lax.axis_index("tp"), 2)
+    own_half = lax.dynamic_slice_in_dim(
+        normed_tokens, part * (model_width // 2), model_width // 2, 1
+    )
+    half_tokens = lax.all_gather(own_half, "ep", axis=0, tiled=True)
+    pairs = [[2 * i, 2 * i + 1] for i in range(lax.axis_size("tp") // 2)]
+    all_tokens = lax.all_gather(
+        half_tokens, "tp", axis=1, tiled=True, axis_index_groups=pairs
+    )
     ssm_out = mixer_local(
         mixer_group_input,
         log_step_size,

time: 235 us -> 228 us (0.970)
  waiting for transfers between devices: 75.7 us -> 65.7 us
    all_gather x1 -> x2, waiting for transfers between devices: 75.6 us -> 65.6 us  [the longest x1 51.9 us: on_device(): half_tokens = lax.all_gather(own_half, 'ep', axis=0, tiled=True)]
  transfers between devices with their start and end apart: 3 -> 4, of which waited for: 1 -> 2; matrix products, arithmetic and copies ran while one was open for 17% -> 17% of each run, Pallas kernels for 7% -> 7%
where the time goes in v2:
time: 228 us; the launch traced here: 227 us
  waiting for transfers between devices  65.7 us (29%)
  blocking collectives  63.4 us (28%)
  local copies, waits for them, and re-layouts  34.7 us (15%)
  matrix products  21.2 us (9%)
  Pallas kernels  16.6 us (7%)
  between operations  14 us (6%)
  starting transfers between devices  6.07 us (3%)
  other arithmetic  5.42 us (2%)
    all_gather x1, waiting for transfers between devices, on_device(): half_tokens = lax.all_gather(own_half, 'ep', axis=0, tiled=True)  51.9 us
    all_gather x1, blocking collectives, mixer_local(): all_ends = lax.all_gather(ends, 'ep')  48.4 us
    broadcast_in_dim x6, local copies, waits for them, and re-layouts, mixer_local(): jnp.where(same[None, :, None, :, None], group_out.transpose(0, 1, 3, 2)[:...  14.4 us
    all_gather x1, waiting for transfers between devices, on_device(): lax.all_gather(half_tokens, 'tp', axis=1, tiled=True, axis_index_groups=p...  13.7 us
    pallas_call x1, Pallas kernels, mixer_local(): pl.pallas_call(scan_kernel, grid=(tiles,), in_specs=[whole_u, pl.BlockSpe...  9.21 us
    all_gather x1, blocking collectives, on_device(): whole_shared = lax.all_gather(shared_hidden, 'tp', axis=1, tiled=True)  7.73 us
    pallas_call x1, Pallas kernels, mixer_local(): pl.pallas_call(lambda *refs: read_kernel(hops, *refs), grid=(tiles,), in_...  7.42 us
    all_gather x1, blocking collectives, on_device(): whole_rows = lax.all_gather(ssm_out, 'tp', axis=1, tiled=True)  7.28 us
  transfers between devices with their start and end apart: 4, of which 2 were waited for; matrix products, arithmetic and copies ran while one was open for 17% of the time, Pallas kernels for 7%

profile of v2, /device:TPU:0, one launch (start us, length us, event | category | flops | bytes accessed | tf_op | source)
XLA Modules:
  0.0 227.0 jit_solution(16338142779001281035)
XLA Ops:
  7.2 0.0 copy-start
  7.2 0.0 all-gather.5.cloned.1.call-start
  7.2 1.4 fusion.16
  8.6 1.2 fusion.18
  9.9 0.8 copy-done.2
  10.7 0.7 constant_dynamic-slice_fusion
  11.4 0.0 all-gather.5.cloned.1.call-update
  11.4 0.0 all-gather.7.cloned.1.call-start
  11.5 51.9 %all-gather.5.cloned.1.call-done = bf16[1024,1024]{1,0:T(8,128)(2,1)} async-done(((bf16[128,1024]{1,0:T(8,128)(2,1)}), bf16[1024,1024]{1,0:T(8,128)(2,1)}) %all-gather.5.cloned.1.call-update) | async-done | bytes 2097168 | tf_op jit(solution)/shard_map/all_gather | solution.py:285
  63.4 0.0 all-gather.7.cloned.1.call-update
  63.4 0.0 all-gather.9.cloned.1.call-start
  63.5 13.7 %all-gather.7.cloned.1.call-done = bf16[1024,2048]{1,0:T(8,128)(2,1)} async-done(((bf16[1024,1024]{1,0:T(8,128)(2,1)}), bf16[1024,2048]{1,0:T(8,128)(2,1)}) %all-gather.7.cloned.1.call-update) | async-done | bytes 4194320 | tf_op jit(solution)/shard_map/all_gather | solution.py:287
  77.2 0.0 copy-done
  77.2 4.7 %fusion.2 = f32[1024,512]{1,0:T(8,128)S(1)} fusion(bf16[1024,2048]{1,0:T(8,128)(2,1)} %all-gather.7.cloned.1.call-done, bf16[1,2048,512]{2,1,0:T(8,128)(2,1)S(1)} %copy-done), kind=kOutput, calls=%fused_computation.2 | convolution fusion | flops 2147483648 | bytes 8388608 | tf_op jit(solution)/shard_map/dot_general | solution.py:245
  81.8 0.0 copy-done.13
  81.8 0.0 copy-done.14
  81.8 3.6 %multiply_convert_fusion = bf16[1024,512]{1,0:T(8,128)(2,1)} fusion(f32[1024,512]{1,0:T(8,128)S(1)} %fusion.2, bf16[1024,2048]{1,0:T(8,128)(2,1)S(1)} %copy-done.13, bf16[1,2048,512]{2,1,0:T(8,128)(2,1)S(1)} %copy-done.14), kind=kOutput, calls=%fused_computation.7 | convolution fusion | flops 2150629376 | bytes 9437184 | tf_op jit(solution)/shard_map/dot_general | solution.py:244
  85.5 0.0 all-gather.9.cloned.1.call-update
  85.5 0.6 copy-done.8
  86.1 0.1 copy.51
  86.2 0.2 broadcast_in_dim.76
  86.4 0.8 broadcast_in_dim.77
  87.2 0.0 copy-done.5
  87.2 1.7 broadcast_in_dim.79
  88.9 3.3 %broadcast_in_dim.80 = bf16[2,256,1024]{2,1,0:T(8,128)(2,1)S(1)} reshape(bf16[2,16,16,16,64]{4,3,2,1,0:T(8,128)(2,1)} %broadcast_in_dim.79) | data formatting | bytes 2097152 | tf_op jit(solution)/shard_map/jit(_where)/broadcast_in_dim | solution.py:174
  92.2 0.7 copy.61
  92.9 0.7 exponential_bitcast_fusion
  93.6 0.1 reshape.72
  93.7 0.8 copy.52
  94.6 1.1 reshape_reshape.6
  95.7 1.4 copy.53
  97.1 0.1 reshape.73
  97.2 0.8 copy.54
  98.0 1.1 reshape_reshape.7
  99.1 1.4 copy.55
  100.6 1.4 reshape.74.eig_ref
  101.9 1.4 reshape.75.freq_ref
  103.3 1.7 broadcast_in_dim.82
  105.0 2.5 %broadcast_in_dim.83 = pred[1024,256]{0,1:T(8,128)(4,1)} reshape(pred[16,64,16,16]{1,0,3,2:T(8,128)(4,1)} %broadcast_in_dim.82) | data formatting | bytes 524288 | tf_op jit(solution)/shard_map/jit(_where)/broadcast_in_dim | solution.py:177
  107.5 2.0 copy.56
  109.5 1.8 broadcast_in_dim.85
  111.3 4.1 %broadcast_in_dim.86 = bf16[2,1024,256]{1,2,0:T(8,128)(2,1)} reshape(bf16[2,16,64,16,16]{2,1,4,3,0:T(8,128)(2,1)} %broadcast_in_dim.85) | data formatting | bytes 2097152 | tf_op jit(solution)/shard_map/jit(_where)/broadcast_in_dim | solution.py:177
  115.4 2.3 %copy.58 = bf16[2,1024,256]{2,1,0:T(8,128)(2,1)} copy(bf16[2,1024,256]{1,2,0:T(8,128)(2,1)} %broadcast_in_dim.86) | data formatting | bytes 2097152 | tf_op jit(solution)/shard_map/jit(_where)/broadcast_in_dim | solution.py:177
  117.7 1.2 broadcast_select_fusion.1.win_ref
  118.9 9.2 %scan_states.1 = (f32[256,1024]{1,0:T(8,128)}, f32[256,1024]{1,0:T(8,128)}, f32[256,1024]{1,0:T(8,128)}, f32[256,1024]{1,0:T(8,128)}, f32[8,4,128]{2,1,0:T(4,128)}) custom-call(bf16[256,256]{1,0:T(8,128)(2,1)} %bitcast.68, bf16[2,256,1024]{2,1,0:T(8,128)(2,1)} %broadcast_select_fusion.1.win_ref, f32[8,256,2]{2,1,0:T(8,128)} %bitcast.66, ...), custom_call_target="tpu_custom_call" | custom-call | flops 268435456 | bytes 6291456 | tf_op jit(solution)/shard_map/scan_states/pallas_call | solution.py:186
  128.1 1.2 broadcast_select_fusion.refs_5_
  129.3 6.2 %fusion.8 = bf16[1024,512]{1,0:T(8,128)(2,1)} fusion(bf16[1024,2048]{1,0:T(8,128)(2,1)} %all-gather.9.cloned.1.call-done, bf16[1,2048,512]{2,1,0:T(8,128)(2,1)} %param.36), kind=kOutput, calls=%fused_computation.8 | convolution fusion | flops 2148007936 | bytes 7340032 | tf_op jit(solution)/shard_map/dot_general | solution.py:313
  135.5 6.0 %all-to-all-start = ((bf16[8,128,512]{2,1,0:T(8,128)(2,1)}), bf16[8,128,512]{2,1,0:T(8,128)(2,1)S(1)}, u32[]{:S(2)}, u32[]{:S(2)}) async-start(bf16[8,128,512]{2,1,0:T(8,128)(2,1)} %bitcast.72), calls=%async_computation | async-start | bytes 2097152 | tf_op jit(solution)/shard_map/all_to_all | solution.py:317
  141.4 0.0 copy-done.10
  141.4 48.4 %all-gather = f32[64,4,128]{2,1,0:T(4,128)} all-gather(f32[8,4,128]{2,1,0:T(4,128)S(1)} %copy-done.10), channel_id=2, replica_groups=mesh['ep'=8,'tp'=4] {'ep'}, dimensions={0}, use_global_device_ids=true | all-gather | bytes 147456 | tf_op jit(solution)/shard_map/all_gather | solution.py:214
  189.8 7.4 %read_states.1 = bf16[256,256]{1,0:T(8,128)(2,1)} custom-call(f32[8,8,4,128]{3,2,1,0:T(4,128)} %bitcast.73, f32[256,1024]{1,0:T(8,128)} %get-tuple-element.8.refs_1_, f32[256,1024]{1,0:T(8,128)} %get-tuple-element.9.refs_2_, f32[256,1024]{1,0:T(8,128)} %get-tuple-element.10.refs_3_, f32[256,1024]{1,0:T(8,128)} %get-tuple-element.11.refs_4_, ...), custom_call_target="tpu_custom_call" | custom-call | flops 536870912 | bytes 6291456 | tf_op jit(solution)/shard_map/read_states/pallas_call | solution.py:215
  197.2 0.9 copy.59
  198.2 0.0 copy-start.15
  198.2 7.3 %all_gather.23 = bf16[256,1024]{1,0:T(8,128)(2,1)S(1)} all-gather(bf16[256,256]{1,0:T(8,128)(2,1)S(1)} %bitcast.75), channel_id=1, replica_groups=mesh['ep'=8,'tp'=4] {'tp'}, dimensions={1}, use_global_device_ids=true | all-gather | bytes 655360 | tf_op jit(solution)/shard_map/all_gather | solution.py:301
  205.5 0.2 fusion.13
  205.7 2.2 fusion.22
  207.9 0.0 copy-start.16
  207.9 0.0 copy-start.17
  207.9 0.5 fusion.11
  208.4 7.7 %all_gather.24 = bf16[128,2048]{1,0:T(8,128)(2,1)} all-gather(bf16[128,512]{1,0:T(8,128)(2,1)S(1)} %fusion.11), channel_id=1, replica_groups=mesh['ep'=8,'tp'=4] {'tp'}, dimensions={1}, use_global_device_ids=true | all-gather | bytes 655360 | tf_op jit(solution)/shard_map/all_gather | solution.py:302
  216.2 1.2 convolution_convert_fusion
  217.4 0.0 all-to-all-done
  217.4 0.3 multiply_reduce_fusion
  217.6 2.9 %fusion.12 = bf16[128,512]{1,0:T(8,128)(2,1)} fusion(f32[128,512]{1,0:T(8,128)S(1)} %multiply_reduce_fusion, bf16[128,2048]{1,0:T(8,128)(2,1)} %all_gather.24, bf16[2048,512]{1,0:T(8,128)(2,1)} %param.39), kind=kOutput, calls=%fused_computation.17 | convolution fusion | flops 268566528 | bytes 3014656 | tf_op jit(solution)/shard_map/dot_general | solution.py:309
  (31 shorter events, 0.1 us)
Async XLA Ops:
  7.2 70.0 %copy-start = (bf16[1,2048,512]{2,1,0:T(8,128)(2,1)S(1)}, bf16[1,2048,512]{2,1,0:T(8,128)(2,1)}, u32[]{:S(2)}) copy-start(bf16[1,2048,512]{2,1,0:T(8,128)(2,1)} %param.35) | copy-start | bytes 6291460
  7.2 56.2 %all-gather.5.cloned.1.call-start = ((), (), s32[]{:S(2)}) async-start(), calls=%async_computation.1 | async-start | bytes 2359296 | tf_op jit(solution)/shard_map/all_gather | solution.py:285
  9.8 0.8 copy-start.2
  11.4 65.7 %all-gather.7.cloned.1.call-start = ((), (), s32[]{:S(2)}) async-start(), calls=%async_computation.2 | async-start | bytes 6291456 | tf_op jit(solution)/shard_map/all_gather | solution.py:287
  63.4 65.9 %all-gather.9.cloned.1.call-start = ((), (), s32[]{:S(2)}) async-start(), calls=%async_computation.3 | async-start | bytes 5242880 | tf_op jit(solution)/shard_map/all_gather | solution.py:304
  77.2 4.7 %copy-start.13 = (bf16[1024,2048]{1,0:T(8,128)(2,1)S(1)}, bf16[1024,2048]{1,0:T(8,128)(2,1)}, u32[]{:S(2)}) copy-start(bf16[1024,2048]{1,0:T(8,128)(2,1)} %all-gather.7.cloned.1.call-done) | copy-start | bytes 12582916
  77.2 4.7 %copy-start.14 = (bf16[1,2048,512]{2,1,0:T(8,128)(2,1)S(1)}, bf16[1,2048,512]{2,1,0:T(8,128)(2,1)}, u32[]{:S(2)}) copy-start(bf16[1,2048,512]{2,1,0:T(8,128)(2,1)} %param.34) | copy-start | bytes 6291460
  85.5 1.7 copy-start.5
  85.5 0.6 copy-start.8
  88.9 3.3 %copy-start.6 = (bf16[256,256]{1,0:T(8,128)(2,1)S(1)}, bf16[256,256]{1,0:T(8,128)(2,1)}, u32[]{:S(2)}) copy-start(bf16[256,256]{1,0:T(8,128)(2,1)} %param.20) | copy-start | bytes 393220
  88.9 8.2 %copy-start.9 = (f32[16,256]{1,0:T(8,128)S(1)}, f32[16,256]{1,0:T(8,128)}, u32[]{:S(2)}) copy-start(f32[16,256]{1,0:T(8,128)} %param.22) | copy-start | bytes 49156
  98.0 11.4 %copy-start.7 = (bf16[2,16,16,64]{3,2,1,0:T(8,128)(2,1)S(1)}, bf16[2,16,16,64]{3,2,1,0:T(8,128)(2,1)}, u32[]{:S(2)}) copy-start(bf16[2,16,16,64]{3,2,1,0:T(8,128)(2,1)} %param.26) | copy-start | bytes 196612
  118.9 9.2 %copy-start.1 = (bf16[2,1024,256]{2,1,0:T(8,128)(2,1)S(1)}, bf16[2,1024,256]{2,1,0:T(8,128)(2,1)}, u32[]{:S(2)}) copy-start(bf16[2,1024,256]{2,1,0:T(8,128)(2,1)} %copy.58) | copy-start | bytes 3145732
  118.9 9.2 %copy-start.4 = (pred[1024,256]{1,0:T(8,128)(4,1)S(1)}, pred[1024,256]{1,0:T(8,128)(4,1)}, u32[]{:S(2)}) copy-start(pred[1024,256]{1,0:T(8,128)(4,1)} %copy.56) | copy-start | bytes 786436
  135.5 6.0 %copy-start.10 = (f32[8,4,128]{2,1,0:T(4,128)S(1)}, f32[8,4,128]{2,1,0:T(4,128)}, u32[]{:S(2)}) copy-start(f32[8,4,128]{2,1,0:T(4,128)} %get-tuple-element.7) | copy-start | bytes 49156
  135.5 81.9 %all-to-all-start = ((bf16[8,128,512]{2,1,0:T(8,128)(2,1)}), bf16[8,128,512]{2,1,0:T(8,128)(2,1)S(1)}, u32[]{:S(2)}, u32[]{:S(2)}) async-start(bf16[8,128,512]{2,1,0:T(8,128)(2,1)} %bitcast.72), calls=%async_computation | async-start | bytes 2097152 | tf_op jit(solution)/shard_map/all_to_all | solution.py:317
  189.8 8.4 %copy-start.11 = (f32[128,4]{0,1:T(4,128)S(1)}, f32[128,4]{0,1:T(4,128)}, u32[]{:S(2)}) copy-start(f32[128,4]{0,1:T(4,128)} %param.33) | copy-start | bytes 6148
  189.8 8.4 %copy-start.12 = (s32[128,4]{0,1:T(4,128)S(1)}, s32[128,4]{0,1:T(4,128)}, u32[]{:S(2)}) copy-start(s32[128,4]{0,1:T(4,128)} %param.32) | copy-start | bytes 6148
  198.2 9.7 %copy-start.3 = (bf16[128,2048]{1,0:T(8,128)(2,1)S(1)}, bf16[128,2048]{1,0:T(8,128)(2,1)}, u32[]{:S(2)}) copy-start(bf16[128,2048]{1,0:T(8,128)(2,1)} %copy-done.2) | copy-start | bytes 1572868
  198.2 9.7 %copy-start.15 = (bf16[2048,512]{1,0:T(8,128)(2,1)S(1)}, bf16[2048,512]{1,0:T(8,128)(2,1)}, u32[]{:S(2)}) copy-start(bf16[2048,512]{1,0:T(8,128)(2,1)} %param.38) | copy-start | bytes 6291460
  207.9 8.2 %copy-start.16 = (bf16[1024,512]{1,0:T(8,128)(2,1)S(1)}, bf16[1024,512]{1,0:T(8,128)(2,1)}, u32[]{:S(2)}) copy-start(bf16[1024,512]{1,0:T(8,128)(2,1)} %param.29) | copy-start | bytes 3145732
  207.9 8.2 %copy-start.17 = (f32[1024]{0:T(1024)S(1)}, f32[1024]{0:T(1024)}, u32[]{:S(2)}) copy-start(f32[1024]{0:T(1024)} %param.28) | copy-start | bytes 12292
Sparse Core Ops, SparseCore 0:
  11.5 51.7 all-gather.4
  64.9 12.1 all-gather.6
  85.6 35.6 all-gather.8
